TPU v7x, 128 devices: a whole 4x4x4 slice. The times are simulated.
128 devices in a mesh: rep: 16 (over z, x), fs: 4 (over y), tp: 2 (over core).
Axes of the slice: x: 4, y: 4, z: 4, core: 2. Of those that a mesh axis runs over, the one named last changes fastest.
Arguments:
- inputs: bfloat16 [16384, 2048], P(('rep', 'fs', 'tp')), may hold values from -6 to 6
- out_grad: bfloat16 [16384, 2048], P(('rep', 'fs', 'tp')), may hold values from -24 to 24
- pre_act: bfloat16 [16384, 8192], P('rep', ('fs', 'tp')), may hold values from -6 to 6
- w_up: bfloat16 [2048, 8192], P('rep', ('fs', 'tp')), may hold values from -0.125 to 0.125
- w_down_t: bfloat16 [2048, 8192], P('rep', ('fs', 'tp')), may hold values from -0.0625 to 0.0625
Outputs:
- grad_in: bfloat16 [16384, 2048], P(('rep', 'fs', 'tp'))
- grad_up: float32 [2048, 8192], P('rep', ('fs', 'tp'))
- grad_down_t: float32 [2048, 8192], P('rep', ('fs', 'tp'))
All inputs are finite; a program needn't handle non-finite values.
Results may differ from a plain program's by a relative error of at most 0.014.
Values may be sent and summed in bfloat16 or wider, within the bound.
A program may use at most 128 MiB of HBM per device.

v0:
```python
import jax
import jax.numpy as jnp
from jax import lax
from jax.sharding import PartitionSpec as P


def side_by_side(arrays, axis, dim, along):
    widths = [a.shape[along] for a in arrays]
    both = jnp.concatenate(arrays, axis=along)
    out = lax.all_gather(both, axis, axis=dim, tiled=True)
    return tuple(jnp.split(out, [sum(widths[:k]) for k in range(1, len(widths))], axis=along))


def cut_along(shard, dim, length):
    shape = shard.shape
    tiles = shard.reshape(*shape[:dim], length, shape[dim] // length, *shape[dim + 1 :])
    return jnp.moveaxis(tiles, dim, 0)


def sent_and_summed(shard, axis, dim):
    tiles = cut_along(shard, dim, lax.axis_size(axis))
    arrived = lax.all_to_all(tiles, axis, split_axis=0, concat_axis=0, tiled=True)
    return arrived.astype(jnp.float32).sum(axis=0)


def on_device(inputs, out_grad, pre_act, w_up, w_down_t):
    input_rows, grad_rows = side_by_side((inputs, out_grad), ("fs", "tp"), 0, 1)
    row_count, col_count = pre_act.shape
    pre_float = pre_act.astype(jnp.float32)
    linear = jnp.maximum(pre_float, 0.0)
    squared = (linear * linear).astype(jnp.bfloat16)
    grad_squared = jnp.dot(
        grad_rows,
        lax.all_gather(w_down_t, "rep", axis=0, tiled=True),
        preferred_element_type=jnp.float32,
    )
    grad_pre = (grad_squared * 2.0 * linear).astype(jnp.bfloat16)
    partial_terms = lax.dot_general(
        grad_pre,
        lax.all_gather(w_up, "rep", axis=0, tiled=True),
        (((1,), (1,)), ((), ())),
        preferred_element_type=jnp.float32,
    ).astype(jnp.bfloat16)
    grad_in = sent_and_summed(
        partial_terms.astype(jnp.float32).astype(jnp.bfloat16), ("fs", "tp"), 0
    ).astype(jnp.bfloat16)
    total_tokens = row_count * lax.axis_size("rep")
    factor = float(total_tokens) ** (-0.5)
    down_part = lax.dot_general(
        grad_rows, squared, (((0,), (0,)), ((), ())), preferred_element_type=jnp.float32
    )
    up_part = lax.dot_general(
        input_rows, grad_pre, (((0,), (0,)), ((), ())), preferred_element_type=jnp.float32
    )
    stacked = lax.psum_scatter(
        (jnp.concatenate([down_part, up_part], axis=1) * factor).astype(jnp.bfloat16),
        "rep",
        scatter_dimension=0,
        tiled=True,
    ).astype(jnp.float32)
    grad_down_t = stacked[:, :col_count]
    grad_up = stacked[:, col_count:]
    return (grad_in, grad_up, grad_down_t)


def solution(mesh):
    in_specs = (
        P(("rep", "fs", "tp"), None),
        P(("rep", "fs", "tp"), None),
        P("rep", ("fs", "tp")),
        P("rep", ("fs", "tp")),
        P("rep", ("fs", "tp")),
    )
    out_specs = (P(("rep", "fs", "tp"), None), P("rep", ("fs", "tp")), P("rep", ("fs", "tp")))
    return jax.shard_map(
        on_device, mesh=mesh, in_specs=in_specs, out_specs=out_specs, check_vma=False
    )
```

profile of v0, /device:TPU:0, one launch (start us, length us, event | category | flops | bytes accessed | tf_op | source)
XLA Modules:
  0.0 267.7 jit_solution(14350902395174839867)
XLA Ops:
  7.2 0.0 all-gather.4.cloned.1.call-start
  7.2 2.4 pad_maximum_fusion
  9.6 0.0 all-gather.6.cloned.1.call-start
  9.6 0.7 all-gather.6.cloned.1.call-update
  10.3 0.0 all-gather.8.cloned.1.call-start
  10.4 0.7 all-gather.8.cloned.1.call-update
  11.1 0.0 reduce-scatter.4.cloned.1.call-start
  11.1 50.8 %all-gather.4.cloned.1.call-done = bf16[1024,4096]{1,0:T(8,128)(2,1)} async-done(((bf16[128,4096]{1,0:T(8,128)(2,1)}), bf16[1024,4096]{1,0:T(8,128)(2,1)}) %all-gather.4.cloned.1.call-update) | async-done | bytes 8388624 | tf_op jit(solution)/shard_map/all_gather | solution.py:10
  61.9 10.7 %fusion.3 = f32[2048,1024]{0,1:T(8,128)} fusion(bf16[1024,4096]{1,0:T(8,128)(2,1)} %all-gather.4.cloned.1.call-done, bf16[1024,1024]{1,0:T(8,128)(2,1)} %param.7), kind=kOutput, calls=%fused_computation.8 | convolution fusion | flops 4299161600 | bytes 14680064 | tf_op jit(solution)/shard_map/dot_general | solution.py:49
  72.6 43.1 %all-gather.6.cloned.1.call-done = bf16[2048,1024]{1,0:T(8,128)(2,1)} async-done(((bf16[128,1024]{1,0:T(8,128)(2,1)}), bf16[2048,1024]{1,0:T(8,128)(2,1)}) %all-gather.6.cloned.1.call-update) | async-done | bytes 4194320 | tf_op jit(solution)/shard_map/all_gather | solution.py:34
  115.7 8.1 %multiply_convert_fusion.1 = bf16[1024,1024]{1,0:T(8,128)(2,1)S(1)} fusion(bf16[1024,1024]{1,0:T(8,128)(2,1)S(1)} %copy-done.1, bf16[2048,1024]{1,0:T(8,128)(2,1)} %all-gather.6.cloned.1.call-done, bf16[1024,4096]{1,0:T(8,128)(2,1)} %all-gather.4.cloned.1.call-done), kind=kOutput, calls=%fused_computation.5 | convolution fusion | flops 4300210176 | bytes 12582912 | tf_op jit(solution)/shard_map/dot_general | solution.py:32
  123.9 4.9 %fusion.1 = f32[2048,1024]{0,1:T(8,128)S(1)} fusion(bf16[1024,1024]{1,0:T(8,128)(2,1)S(1)} %multiply_convert_fusion.1, bf16[1024,4096]{1,0:T(8,128)(2,1)S(1)} %copy-done), kind=kOutput, calls=%fused_computation.2 | convolution fusion | flops 4294967296 | bytes 14680064 | tf_op jit(solution)/shard_map/dot_general | solution.py:52
  128.8 4.8 %fusion = bf16[2048,2048]{0,1:T(8,128)(2,1)} fusion(f32[2048,1024]{0,1:T(8,128)S(1)} %fusion.1, f32[2048,1024]{0,1:T(8,128)S(1)} %bitcast.7), kind=kLoop, calls=%fused_computation.1 | loop fusion | flops 12582912 | bytes 25165824 | tf_op jit(solution)/shard_map/convert_element_type | solution.py:56
  133.6 12.4 %copy.12 = bf16[2048,2048]{1,0:T(8,128)(2,1)} copy(bf16[2048,2048]{0,1:T(8,128)(2,1)} %fusion) | data formatting | bytes 16777216
  146.0 0.0 reduce-scatter.4.cloned.1.call-update
  146.0 22.9 %all-gather.8.cloned.1.call-done = bf16[2048,1024]{1,0:T(8,128)(2,1)} async-done(((bf16[128,1024]{1,0:T(8,128)(2,1)}), bf16[2048,1024]{1,0:T(8,128)(2,1)}) %all-gather.8.cloned.1.call-update) | async-done | bytes 4194320 | tf_op jit(solution)/shard_map/all_gather | solution.py:40
  169.0 6.9 %convolution_convert_fusion = bf16[1024,2048]{1,0:T(8,128)(2,1)S(1)} fusion(bf16[1024,1024]{1,0:T(8,128)(2,1)S(1)} %copy-done.3, bf16[2048,1024]{1,0:T(8,128)(2,1)} %all-gather.8.cloned.1.call-done), kind=kOutput, calls=%fused_computation.7 | convolution fusion | flops 4297064448 | bytes 10485760 | tf_op jit(solution)/shard_map/dot_general | solution.py:38
  175.9 53.9 %all_to_all.5 = bf16[8,128,2048]{2,1,0:T(8,128)(2,1)} all-to-all(bf16[8,128,2048]{2,1,0:T(8,128)(2,1)S(1)} %bitcast.8), channel_id=1, replica_groups=mesh['rep'=16,'fs'=4,'tp'=2] {'fs','tp'}, dimensions={0} | all-to-all | bytes 8388608 | tf_op jit(solution)/shard_map/all_to_all | solution.py:22
  229.8 3.9 %reduce_sum.12 = bf16[128,2048]{1,0:T(8,128)(2,1)} reduce(bf16[8,128,2048]{2,1,0:T(8,128)(2,1)} %all_to_all.5, bf16[]{:T(256)} %constant.3.clone.1), dimensions={0}, to_apply=%region_0.0 | reduce | flops 1835008 | bytes 4718594 | tf_op jit(solution)/shard_map/reduce_sum | solution.py:23
  233.6 24.1 %reduce-scatter.4.cloned.1.call-done = bf16[128,2048]{1,0:T(8,128)(2,1)} async-done(((bf16[2048,2048]{1,0:T(8,128)(2,1)}), bf16[128,2048]{1,0:T(8,128)(2,1)}) %reduce-scatter.4.cloned.1.call-update) | async-done | bytes 524304
  257.8 1.3 copy.13
  259.1 0.1 fusion.11
  259.2 1.0 copy.11
  260.2 1.0 copy.10
  (14 shorter events, 0.0 us)
Async XLA Ops:
  7.2 54.7 %all-gather.4.cloned.1.call-start = ((), (), s32[]{:S(2)}) async-start(), calls=%async_computation.2 | async-start | bytes 9437184 | tf_op jit(solution)/shard_map/all_gather | solution.py:10
  9.6 106.1 %all-gather.6.cloned.1.call-start = ((), (), s32[]{:S(2)}) async-start(), calls=%async_computation.3 | async-start | bytes 4456448 | tf_op jit(solution)/shard_map/all_gather | solution.py:34
  10.3 158.6 %all-gather.8.cloned.1.call-start = ((), (), s32[]{:S(2)}) async-start(), calls=%async_computation.4 | async-start | bytes 4456448 | tf_op jit(solution)/shard_map/all_gather | solution.py:40
  11.1 104.6 %copy-start.1 = (bf16[1024,1024]{1,0:T(8,128)(2,1)S(1)}, bf16[1024,1024]{1,0:T(8,128)(2,1)}, u32[]{:S(2)}) copy-start(bf16[1024,1024]{1,0:T(8,128)(2,1)} %param.7) | copy-start | bytes 6291460
  11.1 246.7 %reduce-scatter.4.cloned.1.call-start = ((), (), s32[]{:S(2)}) async-start(), calls=%async_computation.5 | async-start | bytes 8912896
  115.7 8.1 %copy-start = (bf16[1024,4096]{1,0:T(8,128)(2,1)S(1)}, bf16[1024,4096]{1,0:T(8,128)(2,1)}, u32[]{:S(2)}) copy-start(bf16[1024,4096]{1,0:T(8,128)(2,1)} %all-gather.4.cloned.1.call-done) | copy-start | bytes 25165828
  115.7 13.1 %slice-start = ((s8[8388608]{0:T(1024)(128)(4,1)}), s8[4194304]{0:T(1024)(128)(4,1)S(1)}, s32[]{:S(2)}) async-start(s8[8388608]{0:T(1024)(128)(4,1)} %bitcast.6), calls=%async_computation.6 | async-start | bytes 8388608
  123.8 5.0 %copy-start.2 = (bf16[1024,1024]{1,0:T(8,128)(2,1)}, bf16[1024,1024]{1,0:T(8,128)(2,1)S(1)}, u32[]{:S(2)}) copy-start(bf16[1024,1024]{1,0:T(8,128)(2,1)S(1)} %multiply_convert_fusion.1) | copy-start | bytes 6291460
  123.8 5.0 %slice-start.1 = ((s8[8388608]{0:T(1024)(128)(4,1)}), s8[4194304]{0:T(1024)(128)(4,1)S(1)}, s32[]{:S(2)}) async-start(s8[8388608]{0:T(1024)(128)(4,1)} %bitcast.6), calls=%async_computation.7 | async-start | bytes 8388608
  146.0 23.0 %copy-start.3 = (bf16[1024,1024]{1,0:T(8,128)(2,1)S(1)}, bf16[1024,1024]{1,0:T(8,128)(2,1)}, u32[]{:S(2)}) copy-start(bf16[1024,1024]{1,0:T(8,128)(2,1)} %copy-done.2) | copy-start | bytes 6291460
Sparse Core Ops, SparseCore 0:
  9.7 52.1 all-gather.3
  64.0 51.6 all-gather.5
  117.9 51.0 all-gather.7
  172.2 85.5 reduce-scatter.3
where the time goes:
time: 268 us
  waiting for transfers between devices  142 us (53%)
  blocking collectives  53.9 us (20%)
  matrix products  30.7 us (11%)
  local copies, waits for them, and re-layouts  15.8 us (6%)
  between operations  13.9 us (5%)
  other arithmetic  11 us (4%)
    all_to_all x1, blocking collectives, sent_and_summed(): lax.all_to_all(tiles, axis, split_axis=0, concat_axis=0, tiled=True)  53.9 us
    all_gather x1, waiting for transfers between devices, side_by_side(): out = lax.all_gather(both, axis, axis=dim, tiled=True)  50.8 us
    all_gather x1, waiting for transfers between devices, on_device(): lax.all_gather(w_down_t, 'rep', axis=0, tiled=True)  43.1 us
    unnamed x5, waiting for transfers between devices  25.6 us
    all_gather x1, waiting for transfers between devices, on_device(): lax.all_gather(w_up, 'rep', axis=0, tiled=True)  22.9 us
    unnamed x16, local copies, waits for them, and re-layouts  15.7 us
    dot_general x1, matrix products, on_device(): lax.dot_general(grad_rows, squared, (((0,), (0,)), ((), ())), preferred_e...  10.7 us
    dot_general x1, matrix products, on_device(): jnp.dot(grad_rows, lax.all_gather(w_down_t, 'rep', axis=0, tiled=True), p...  8.1 us
  transfers between devices with their start and end apart: 4, of which 4 were waited for; matrix products, arithmetic and copies ran while one was open for 19% of the time, Pallas kernels for 0%

commit v1 on v0

--- a/solution.py
+++ b/solution.py
@@ -2,6 +2,12 @@
 import jax.numpy as jnp
 from jax import lax
 from jax.sharding import PartitionSpec as P
+
+
+def gather_by_exchange(x, axis, dim):
+    size = lax.axis_size(axis)
+    repeats = [size if d == dim else 1 for d in range(x.ndim)]
+    return lax.all_to_all(jnp.tile(x, repeats), axis, split_axis=dim, concat_axis=dim, tiled=True)
 
 
 def side_by_side(arrays, axis, dim, along):
@@ -37,7 +43,7 @@
     grad_pre = (grad_squared * 2.0 * linear).astype(jnp.bfloat16)
     partial_terms = lax.dot_general(
         grad_pre,
-        lax.all_gather(w_up, "rep", axis=0, tiled=True),
+        gather_by_exchange(w_up, "rep", 0),
         (((1,), (1,)), ((), ())),
         preferred_element_type=jnp.float32,
     ).astype(jnp.bfloat16)

time: 268 us -> 293 us (1.093)
  blocking collectives: 53.9 us -> 126 us
  waiting for transfers between devices: 142 us -> 95.4 us
    all_to_all x0 -> x1, blocking collectives: none -> 71.4 us  [gather_by_exchange(): lax.all_to_all(jnp.tile(x, repeats), axis, split_axis=dim, concat_axis=di...]
    unnamed x5 -> x4, waiting for transfers between devices: 25.6 us -> 0.73 us
    all_gather x1 -> x0, waiting for transfers between devices: 22.9 us -> none  [on_device(): lax.all_gather(w_up, 'rep', axis=0, tiled=True)]
    unnamed x16 -> x18, local copies, waits for them, and re-layouts: 15.7 us -> 16.6 us
  transfers between devices with their start and end apart: 4 -> 3, of which waited for: 4 -> 2; matrix products, arithmetic and copies ran while one was open for 19% -> 7% of each run, Pallas kernels for 0% -> 0%
where the time goes in v1:
time: 293 us; the launch traced here: 292 us
  blocking collectives  126 us (43%)
  waiting for transfers between devices  95.4 us (33%)
  matrix products  28.5 us (10%)
  local copies, waits for them, and re-layouts  17.2 us (6%)
  between operations  13.9 us (5%)
  other arithmetic  11 us (4%)
    all_to_all x1, blocking collectives, gather_by_exchange(): lax.all_to_all(jnp.tile(x, repeats), axis, split_axis=dim, concat_axis=di...  71.4 us
    all_to_all x1, blocking collectives, sent_and_summed(): lax.all_to_all(tiles, axis, split_axis=0, concat_axis=0, tiled=True)  54.3 us
    all_gather x1, waiting for transfers between devices, side_by_side(): out = lax.all_gather(both, axis, axis=dim, tiled=True)  51.5 us
    all_gather x1, waiting for transfers between devices, on_device(): lax.all_gather(w_down_t, 'rep', axis=0, tiled=True)  43.2 us
    unnamed x18, local copies, waits for them, and re-layouts  16.6 us
    dot_general x1, matrix products, on_device(): lax.dot_general(grad_rows, squared, (((0,), (0,)), ((), ())), preferred_e...  10.7 us
    dot_general x1, matrix products, on_device(): jnp.dot(grad_rows, lax.all_gather(w_down_t, 'rep', axis=0, tiled=True), p...  8.09 us
  transfers between devices with their start and end apart: 3, of which 2 were waited for; matrix products, arithmetic and copies ran while one was open for 7% of the time, Pallas kernels for 0%

profile of v1, /device:TPU:0, one launch (start us, length us, event | category | flops | bytes accessed | tf_op | source)
XLA Modules:
  0.0 291.6 jit_solution(18262853683539552296)
XLA Ops:
  7.2 0.0 all-gather.3.cloned.1.call-start
  7.2 2.4 pad_maximum_fusion
  9.6 0.0 all-gather.3.cloned.1.call-update
  9.6 0.0 all-gather.5.cloned.1.call-start
  9.6 0.7 all-gather.5.cloned.1.call-update
  10.4 0.0 reduce-scatter.4.cloned.1.call-start
  10.4 51.5 %all-gather.3.cloned.1.call-done = bf16[1024,4096]{1,0:T(8,128)(2,1)} async-done(((bf16[128,4096]{1,0:T(8,128)(2,1)}), bf16[1024,4096]{1,0:T(8,128)(2,1)}) %all-gather.3.cloned.1.call-update) | async-done | bytes 8388624 | tf_op jit(solution)/shard_map/all_gather | solution.py:16
  61.9 10.7 %fusion.3 = f32[2048,1024]{0,1:T(8,128)} fusion(bf16[1024,4096]{1,0:T(8,128)(2,1)} %all-gather.3.cloned.1.call-done, bf16[1024,1024]{1,0:T(8,128)(2,1)} %param.7), kind=kOutput, calls=%fused_computation.8 | convolution fusion | flops 4299161600 | bytes 14680064 | tf_op jit(solution)/shard_map/dot_general | solution.py:55
  72.6 43.2 %all-gather.5.cloned.1.call-done = bf16[2048,1024]{1,0:T(8,128)(2,1)} async-done(((bf16[128,1024]{1,0:T(8,128)(2,1)}), bf16[2048,1024]{1,0:T(8,128)(2,1)}) %all-gather.5.cloned.1.call-update) | async-done | bytes 4194320 | tf_op jit(solution)/shard_map/all_gather | solution.py:40
  115.7 8.1 %multiply_convert_fusion.1 = bf16[1024,1024]{1,0:T(8,128)(2,1)S(1)} fusion(bf16[1024,1024]{1,0:T(8,128)(2,1)S(1)} %copy-done.2, bf16[2048,1024]{1,0:T(8,128)(2,1)} %all-gather.5.cloned.1.call-done, bf16[1024,4096]{1,0:T(8,128)(2,1)} %all-gather.3.cloned.1.call-done), kind=kOutput, calls=%fused_computation.5 | convolution fusion | flops 4300210176 | bytes 12582912 | tf_op jit(solution)/shard_map/dot_general | solution.py:38
  123.9 4.9 %fusion.1 = f32[2048,1024]{0,1:T(8,128)S(1)} fusion(bf16[1024,1024]{1,0:T(8,128)(2,1)S(1)} %multiply_convert_fusion.1, bf16[1024,4096]{1,0:T(8,128)(2,1)S(1)} %copy-done.1), kind=kOutput, calls=%fused_computation.2 | convolution fusion | flops 4294967296 | bytes 14680064 | tf_op jit(solution)/shard_map/dot_general | solution.py:58
  128.9 4.8 %fusion = bf16[2048,2048]{0,1:T(8,128)(2,1)} fusion(f32[2048,1024]{0,1:T(8,128)S(1)} %fusion.1, f32[2048,1024]{0,1:T(8,128)S(1)} %bitcast.8), kind=kLoop, calls=%fused_computation.1 | loop fusion | flops 12582912 | bytes 25165824 | tf_op jit(solution)/shard_map/convert_element_type | solution.py:62
  133.6 12.3 %copy.12 = bf16[2048,2048]{1,0:T(8,128)(2,1)} copy(bf16[2048,2048]{0,1:T(8,128)(2,1)} %fusion) | data formatting | bytes 16777216
  145.9 0.0 reduce-scatter.4.cloned.1.call-update
  146.0 0.9 copy-done
  146.9 0.5 tile.2
  147.4 71.4 %all_to_all.14 = bf16[16,128,1024]{2,1,0:T(8,128)(2,1)S(1)} all-to-all(bf16[16,128,1024]{2,1,0:T(8,128)(2,1)S(1)} %tile.2), channel_id=1, replica_groups=mesh['rep'=16,'fs'=4,'tp'=2] {'rep'}, dimensions={0} | all-to-all | bytes 8388608 | tf_op jit(solution)/shard_map/all_to_all | solution.py:10
  218.8 4.8 %convolution_convert_fusion = bf16[1024,2048]{1,0:T(8,128)(2,1)S(1)} fusion(bf16[1024,1024]{1,0:T(8,128)(2,1)S(1)} %copy-done.4, bf16[2048,1024]{1,0:T(8,128)(2,1)S(1)} %bitcast.9), kind=kOutput, calls=%fused_computation.7 | convolution fusion | flops 4297064448 | bytes 10485760 | tf_op jit(solution)/shard_map/dot_general | solution.py:44
  223.6 54.3 %all_to_all.15 = bf16[8,128,2048]{2,1,0:T(8,128)(2,1)} all-to-all(bf16[8,128,2048]{2,1,0:T(8,128)(2,1)S(1)} %bitcast.10), channel_id=1, replica_groups=mesh['rep'=16,'fs'=4,'tp'=2] {'fs','tp'}, dimensions={0} | all-to-all | bytes 8388608 | tf_op jit(solution)/shard_map/all_to_all | solution.py:28
  277.9 3.8 %reduce_sum.12 = bf16[128,2048]{1,0:T(8,128)(2,1)} reduce(bf16[8,128,2048]{2,1,0:T(8,128)(2,1)} %all_to_all.15, bf16[]{:T(256)} %constant.3.clone.1), dimensions={0}, to_apply=%region_0.0 | reduce | flops 1835008 | bytes 4718594 | tf_op jit(solution)/shard_map/reduce_sum | solution.py:29
  281.7 1.3 copy.13
  283.0 0.1 fusion.11
  283.1 1.0 copy.11
  284.1 1.0 copy.10
  (15 shorter events, 0.0 us)
Async XLA Ops:
  7.2 54.7 %all-gather.3.cloned.1.call-start = ((), (), s32[]{:S(2)}) async-start(), calls=%async_computation.3 | async-start | bytes 9437184 | tf_op jit(solution)/shard_map/all_gather | solution.py:16
  9.6 106.1 %all-gather.5.cloned.1.call-start = ((), (), s32[]{:S(2)}) async-start(), calls=%async_computation.4 | async-start | bytes 4456448 | tf_op jit(solution)/shard_map/all_gather | solution.py:40
  10.4 105.4 %copy-start.2 = (bf16[1024,1024]{1,0:T(8,128)(2,1)S(1)}, bf16[1024,1024]{1,0:T(8,128)(2,1)}, u32[]{:S(2)}) copy-start(bf16[1024,1024]{1,0:T(8,128)(2,1)} %param.7) | copy-start | bytes 6291460
  10.4 271.4 %reduce-scatter.4.cloned.1.call-start = ((), (), s32[]{:S(2)}) async-start(), calls=%async_computation.5 | async-start | bytes 8912896
  115.7 8.1 %copy-start.1 = (bf16[1024,4096]{1,0:T(8,128)(2,1)S(1)}, bf16[1024,4096]{1,0:T(8,128)(2,1)}, u32[]{:S(2)}) copy-start(bf16[1024,4096]{1,0:T(8,128)(2,1)} %all-gather.3.cloned.1.call-done) | copy-start | bytes 25165828
  115.7 13.1 %slice-start = ((s8[8388608]{0:T(1024)(128)(4,1)}), s8[4194304]{0:T(1024)(128)(4,1)S(1)}, s32[]{:S(2)}) async-start(s8[8388608]{0:T(1024)(128)(4,1)} %bitcast.7), calls=%async_computation.6 | async-start | bytes 8388608
  123.8 5.0 %copy-start.3 = (bf16[1024,1024]{1,0:T(8,128)(2,1)}, bf16[1024,1024]{1,0:T(8,128)(2,1)S(1)}, u32[]{:S(2)}) copy-start(bf16[1024,1024]{1,0:T(8,128)(2,1)S(1)} %multiply_convert_fusion.1) | copy-start | bytes 6291460
  123.9 5.0 %slice-start.1 = ((s8[8388608]{0:T(1024)(128)(4,1)}), s8[4194304]{0:T(1024)(128)(4,1)S(1)}, s32[]{:S(2)}) async-start(s8[8388608]{0:T(1024)(128)(4,1)} %bitcast.7), calls=%async_computation.7 | async-start | bytes 8388608
  145.9 0.9 copy-start
  147.4 71.4 %copy-start.4 = (bf16[1024,1024]{1,0:T(8,128)(2,1)S(1)}, bf16[1024,1024]{1,0:T(8,128)(2,1)}, u32[]{:S(2)}) copy-start(bf16[1024,1024]{1,0:T(8,128)(2,1)} %copy-done.3) | copy-start | bytes 6291460
Sparse Core Ops, SparseCore 0:
  9.7 52.1 all-gather.2
  64.1 51.6 all-gather.4
  146.1 121.6 reduce-scatter.3
